TPU v7x, 32 devices: a whole 2x2x4 slice. The times are simulated.
32 devices in a mesh: rep: 2 (over x), fs: 8 (over z, y), tp: 2 (over core).
Axes of the slice: x: 2, y: 2, z: 4, core: 2. Of those that a mesh axis runs over, the one named last changes fastest.
Arguments:
- pre_gate: bfloat16 [12288, 4096], P(('rep', 'fs'), 'tp'), may hold values from -6 to 6
- pre_linear: bfloat16 [12288, 4096], P(('rep', 'fs'), 'tp'), may hold values from -6 to 6
- taps_gate: float32 [3, 4096], P(None, 'tp'), may hold values from -3.5 to 3.5
- taps_linear: float32 [3, 4096], P(None, 'tp'), may hold values from -3.5 to 3.5
- bias_gate: float32 [4096], P('tp'), may hold values from -3 to 3
- bias_linear: float32 [4096], P('tp'), may hold values from -3 to 3
- down_weight: bfloat16 [4096, 2048], P('tp', 'fs'), may hold values from -0.09375 to 0.09375
- out_grad: bfloat16 [12288, 2048], P(('rep', 'fs')), may hold values from -8 to 8
Outputs:
- grad_gate: bfloat16 [12288, 4096], P(('rep', 'fs'), 'tp')
- grad_linear: bfloat16 [12288, 4096], P(('rep', 'fs'), 'tp')
- grad_taps_gate: float32 [3, 4096], P(None, 'tp')
- grad_taps_linear: float32 [3, 4096], P(None, 'tp')
- grad_bias_gate: float32 [4096], P('tp')
- grad_bias_linear: float32 [4096], P('tp')
- grad_down: float32 [4096, 2048], P('tp', 'fs')
- row_norms: float32 [4096], P('tp')
All inputs are finite; a program needn't handle non-finite values.
Results may differ from a plain program's by a relative error of at most 0.0031.
Values may be sent and summed in bfloat16 or wider, within the bound.
No kernel may reach another device: no remote copies, remote signals or barrier semaphores. Data moves between devices by JAX's collectives and lax.ppermute only.
A program may use at most 128 MiB of HBM per device.

v0:
```python
import jax
import jax.numpy as jnp
from jax import lax
from jax.sharding import PartitionSpec as P


def convolve(values, taps, bias):
    length = values.shape[0]
    padded = jnp.pad(values, ((2, 0), (0, 0)))
    return (
        taps[0] * padded[0:length]
        + taps[1] * padded[1 : length + 1]
        + taps[2] * padded[2 : length + 2]
        + bias
    )


def convolve_back(grads, taps):
    length = grads.shape[0]
    padded = jnp.pad(grads, ((0, 2), (0, 0)))
    return (
        taps[0] * padded[2 : length + 2]
        + taps[1] * padded[1 : length + 1]
        + taps[2] * padded[0:length]
    )


def tap_grads(grads, values):
    length = values.shape[0]
    padded = jnp.pad(values, ((2, 0), (0, 0)))
    return jnp.stack([jnp.sum(grads * padded[j : j + length], axis=0) for j in range(3)])


def local(
    pre_gate, pre_linear, taps_gate, taps_linear, bias_gate, bias_linear, down_weight, out_grad
):
    gate_in = pre_gate.astype(jnp.float32)
    linear_in = pre_linear.astype(jnp.float32)
    gate_pre = convolve(gate_in, taps_gate, bias_gate)
    linear_pre = convolve(linear_in, taps_linear, bias_linear)
    sigma = jax.nn.sigmoid(gate_pre)
    silu_val = gate_pre * sigma
    hidden = (silu_val * linear_pre).astype(jnp.bfloat16)
    columns = out_grad
    grad_hidden = lax.dot_general(
        columns,
        lax.all_gather(down_weight, "fs", axis=1, tiled=True),
        (((1,), (1,)), ((), ())),
        preferred_element_type=jnp.float32,
    )
    grad_gate_pre = grad_hidden * linear_pre * sigma * (1.0 + gate_pre * (1.0 - sigma))
    grad_linear_pre = grad_hidden * silu_val
    grad_gate = convolve_back(grad_gate_pre, taps_gate).astype(jnp.bfloat16)
    grad_linear = convolve_back(grad_linear_pre, taps_linear).astype(jnp.bfloat16)
    conv_parts = (
        tap_grads(grad_gate_pre, gate_in),
        tap_grads(grad_linear_pre, linear_in),
        jnp.sum(grad_gate_pre, axis=0),
        jnp.sum(grad_linear_pre, axis=0),
    )
    grad_taps_gate, grad_taps_linear, grad_bias_gate, grad_bias_linear = lax.psum(
        (conv_parts[0], conv_parts[1], conv_parts[2], conv_parts[3]), ("rep", "fs")
    )
    columns = out_grad
    partial_grad = lax.psum_scatter(
        lax.dot_general(
            columns, hidden, (((0,), (0,)), ((), ())), preferred_element_type=jnp.float32
        ),
        "fs",
        scatter_dimension=0,
        tiled=True,
    )
    summed = lax.psum(partial_grad, "rep")
    grad_down = summed.T
    row_norms = lax.psum(jnp.sum(grad_down * grad_down, axis=1), "fs")
    return (
        grad_gate,
        grad_linear,
        grad_taps_gate,
        grad_taps_linear,
        grad_bias_gate,
        grad_bias_linear,
        grad_down,
        row_norms,
    )


def solution(mesh):
    in_specs = (
        P(("rep", "fs"), "tp"),
        P(("rep", "fs"), "tp"),
        P(None, "tp"),
        P(None, "tp"),
        P("tp"),
        P("tp"),
        P("tp", "fs"),
        P(("rep", "fs"), None),
    )
    out_specs = (
        P(("rep", "fs"), "tp"),
        P(("rep", "fs"), "tp"),
        P(None, "tp"),
        P(None, "tp"),
        P("tp"),
        P("tp"),
        P("tp", "fs"),
        P("tp"),
    )
    return jax.shard_map(local, mesh=mesh, in_specs=in_specs, out_specs=out_specs, check_vma=False)
```

profile of v0, /device:TPU:0, one launch (start us, length us, event | category | flops | bytes accessed | tf_op | source)
XLA Modules:
  0.0 668.1 jit_solution(7865275278848254621)
XLA Ops:
  7.2 0.0 copy-start
  7.2 0.0 all-gather.2.cloned.1.call-start
  7.2 0.7 all-gather.2.cloned.1.call-update
  7.9 0.0 reduce-scatter.2.cloned.1.call-start
  8.0 0.0 copy-start.3
  8.0 5.6 convert_element_type.24
  13.5 0.0 copy-done.3
  13.5 0.0 copy-start.4
  13.5 0.0 copy-start.5
  13.5 0.0 copy-start.7
  13.5 3.4 convert_element_type.23
  17.0 0.0 copy-done.4
  17.0 0.0 copy-done.5
  17.0 120.7 %all-gather.2.cloned.1.call-done = bf16[2048,2048]{1,0:T(8,128)(2,1)} async-done(((bf16[2048,256]{1,0:T(8,128)(2,1)}), bf16[2048,2048]{1,0:T(8,128)(2,1)}) %all-gather.2.cloned.1.call-update) | async-done | bytes 8388624 | tf_op jit(solution)/shard_map/all_gather | solution.py:47
  137.7 0.0 copy-done
  137.7 0.0 copy-done.7
  137.7 0.0 copy-start.1
  137.7 0.0 copy-start.2
  137.7 0.0 copy-start.6
  137.8 25.9 %fusion.4 = (f32[2048]{0:T(1024)}, f32[2048]{0:T(1024)S(1)}, f32[2048]{0:T(1024)S(1)}, f32[2048]{0:T(1024)S(1)}, f32[768,2048]{1,0:T(8,128)}, /*index=5*/f32[768,2048]{1,0:T(8,128)}, f32[768,2048]{1,0:T(8,128)}) fusion(bf16[768,2048]{1,0:T(8,128)(2,1)} %param.9, f32[768,2048]{1,0:T(8,128)} %convert_element_type.23, f32[2048]{0:T(1024)S(1)} %copy-done.7, ...), kind=kOutput, calls=%fused_computation.24 | convolution fusion | flops 6472327168 | bytes 46202880 | tf_op jit(solution)/shard_map/dot_general | solution.py:45
  163.7 0.0 copy-done.1
  163.7 0.0 copy-done.2
  163.7 0.0 copy-done.6
  163.7 19.0 %fusion.5 = (f32[2048]{0:T(1024)}, f32[2048]{0:T(1024)S(1)}, f32[2048]{0:T(1024)S(1)}, f32[2048]{0:T(1024)S(1)}, f32[768,2048]{1,0:T(8,128)}, /*index=5*/f32[768,2048]{1,0:T(8,128)}, bf16[768,2048]{1,0:T(8,128)(2,1)}) fusion(bf16[768,2048]{1,0:T(8,128)(2,1)} %param.8, f32[768,2048]{1,0:T(8,128)S(1)} %copy-done.1, f32[768,2048]{1,0:T(8,128)} %get-tuple-element.25, ...), kind=kLoop, calls=%fused_computation.25 | loop fusion | flops 45604864 | bytes 50397184 | tf_op jit(solution)/shard_map/reduce_sum | solution.py:58
  182.7 15.2 %convolution_bitcast_fusion = f32[2048,2048]{0,1:T(8,128)} fusion(bf16[768,2048]{1,0:T(8,128)(2,1)S(1)} %copy-done, f32[768,2048]{1,0:T(8,128)} %get-tuple-element.27, f32[768,2048]{1,0:T(8,128)} %get-tuple-element.25), kind=kOutput, calls=%fused_computation | convolution fusion | flops 6451888128 | bytes 32505856 | tf_op jit(solution)/shard_map/dot_general | solution.py:66
  197.8 0.0 reduce-scatter.2.cloned.1.call-update
  197.9 0.0 all-reduce.8.cloned.1.call-start
  197.9 278.5 %reduce-scatter.2.cloned.1.call-done = f32[256,2048]{0,1:T(8,128)} async-done(((f32[2048,2048]{0,1:T(8,128)}), f32[256,2048]{0,1:T(8,128)}) %reduce-scatter.2.cloned.1.call-update) | async-done | bytes 2097168 | tf_op jit(solution)/shard_map/reduce_scatter | solution.py:65
  476.4 0.0 all-reduce.8.cloned.1.call-update
  476.5 0.0 all-reduce.10.cloned.1.call-start
  476.5 0.7 pad_maximum_fusion
  477.2 9.6 %add_convert_fusion.1 = bf16[768,2048]{1,0:T(8,128)(2,1)} fusion(f32[768,2048]{1,0:T(8,128)} %get-tuple-element.26, f32[2048]{0:T(1024)S(1)} %bitcast.28, f32[2048]{0:T(1024)S(1)} %bitcast.30, f32[2048]{0:T(1024)S(1)} %bitcast.26), kind=kLoop, calls=%fused_computation.9 | loop fusion | flops 9437184 | bytes 9461760 | tf_op jit(solution)/shard_map/convert_element_type | solution.py:53
  486.8 0.0 all-reduce.10.cloned.1.call-update
  486.8 54.0 %all-reduce.8.cloned.1.call-done = f32[2048,256]{1,0:T(8,128)} async-done(((f32[2048,256]{1,0:T(8,128)}), f32[2048,256]{1,0:T(8,128)}) %all-reduce.8.cloned.1.call-update) | async-done | bytes 2097168 | tf_op jit(solution)/shard_map/psum | solution.py:73
  540.8 1.9 multiply_reduce_fusion.6
  542.8 22.3 %psum.47 = f32[2048]{0:T(1024)} all-reduce(f32[2048]{0:T(1024)S(1)} %multiply_reduce_fusion.6), channel_id=1, replica_groups=mesh['rep'=2,'fs'=8,'tp'=2] {'fs'}, use_global_device_ids=true, to_apply=%region_15.16 | all-reduce | flops 2048 | bytes 16384 | tf_op jit(solution)/shard_map/psum | solution.py:75
  565.1 88.1 %all-reduce.10.cloned.1.call-done = (f32[3,2048]{1,0:T(4,128)}, f32[3,2048]{1,0:T(4,128)}, f32[2048]{0:T(1024)}, f32[2048]{0:T(1024)}) async-done(((f32[3,2048]{1,0:T(4,128)}, f32[3,2048]{1,0:T(4,128)}, f32[2048]{0:T(1024)}, f32[2048]{0:T(1024)}), (f32[3,2048]{1,0:T(4,128)}, f32[3,2048]{1,0:T(4,128)}, f32[2048]{0:T(1024)}, f32[2048]{0:T(1024)})) %all-reduce.10.cloned.1.call-update) | async-done | bytes 65552 | tf_op jit(solution)/shard_map/psum | solution.py:61
  653.2 1.4 copy.21
  654.6 1.4 copy.22
  655.9 1.3 copy.23
  657.2 1.3 copy.24
  658.5 3.0 copy.25
  (2 shorter events, 0.0 us)
Async XLA Ops:
  7.2 130.6 %copy-start = (bf16[768,2048]{1,0:T(8,128)(2,1)S(1)}, bf16[768,2048]{1,0:T(8,128)(2,1)}, u32[]{:S(2)}) copy-start(bf16[768,2048]{1,0:T(8,128)(2,1)} %param.15) | copy-start | bytes 9437188
  7.2 130.5 %all-gather.2.cloned.1.call-start = ((), (), s32[]{:S(2)}) async-start(), calls=%async_computation.1 | async-start | bytes 9437184 | tf_op jit(solution)/shard_map/all_gather | solution.py:47
  7.9 468.5 %reduce-scatter.2.cloned.1.call-start = ((), (), s32[]{:S(2)}) async-start(), calls=%async_computation.2 | async-start | bytes 18874368 | tf_op jit(solution)/shard_map/reduce_scatter | solution.py:65
  8.0 5.6 copy-start.3
  13.5 3.4 copy-start.4
  13.5 3.5 copy-start.5
  13.5 124.2 %copy-start.7 = (f32[2048]{0:T(1024)S(1)}, f32[2048]{0:T(1024)}, u32[]{:S(2)}) copy-start(f32[2048]{0:T(1024)} %param.12) | copy-start | bytes 24580
  137.7 25.9 %copy-start.1 = (f32[768,2048]{1,0:T(8,128)S(1)}, f32[768,2048]{1,0:T(8,128)}, u32[]{:S(2)}) copy-start(f32[768,2048]{1,0:T(8,128)} %convert_element_type.24) | copy-start | bytes 18874372
  137.7 25.9 %copy-start.2 = (f32[768,2048]{1,0:T(8,128)S(1)}, f32[768,2048]{1,0:T(8,128)}, u32[]{:S(2)}) copy-start(f32[768,2048]{1,0:T(8,128)} %convert_element_type.23) | copy-start | bytes 18874372
  137.7 25.9 %copy-start.6 = (f32[2048]{0:T(1024)S(1)}, f32[2048]{0:T(1024)}, u32[]{:S(2)}) copy-start(f32[2048]{0:T(1024)} %param.13) | copy-start | bytes 24580
  197.9 343.0 %all-reduce.8.cloned.1.call-start = ((), (), s32[]{:S(2)}) async-start(), calls=%async_computation.3 | async-start | bytes 4194304 | tf_op jit(solution)/shard_map/psum | solution.py:73
  476.5 176.7 %all-reduce.10.cloned.1.call-start = ((), (), s32[]{:S(2)}) async-start(), calls=%async_computation.4 | async-start | bytes 163840 | tf_op jit(solution)/shard_map/psum | solution.py:61
Sparse Core Ops, SparseCore 0:
  10.0 127.6 all-gather.1
  198.0 278.3 reduce-scatter.1
  478.7 62.0 all-reduce.7
  547.2 105.9 all-reduce.9
where the time goes:
time: 669 us; the launch traced here: 668 us
  waiting for transfers between devices  542 us (81%)
  matrix products  41.1 us (6%)
  other arithmetic  40.2 us (6%)
  blocking collectives  22.3 us (3%)
  between operations  13.8 us (2%)
  local copies, waits for them, and re-layouts  8.47 us (1%)
    reduce_scatter x1, waiting for transfers between devices, local(): lax.psum_scatter(lax.dot_general(columns, hidden, (((0,), (0,)), ((), ())...  279 us
    all_gather x1, waiting for transfers between devices, local(): lax.all_gather(down_weight, 'fs', axis=1, tiled=True)  121 us
    psum x1, waiting for transfers between devices, local(): lax.psum((conv_parts[0], conv_parts[1], conv_parts[2], conv_parts[3]), ('...  88.1 us
    psum x1, waiting for transfers between devices, local(): summed = lax.psum(partial_grad, 'rep')  54 us
    dot_general x1, matrix products, local(): lax.dot_general(columns, lax.all_gather(down_weight, 'fs', axis=1, tiled=...  25.9 us
    psum x1, blocking collectives, local(): row_norms = lax.psum(jnp.sum(grad_down * grad_down, axis=1), 'fs')  22.3 us
    reduce_sum x1, other arithmetic, local(): jnp.sum(grad_gate_pre, axis=0)  19 us
    dot_general x1, matrix products, local(): lax.dot_general(columns, hidden, (((0,), (0,)), ((), ())), preferred_elem...  15.2 us
  transfers between devices with their start and end apart: 4, of which 4 were waited for; matrix products, arithmetic and copies ran while one was open for 3% of the time, Pallas kernels for 0%

commit v1 on v0

--- a/solution.py
+++ b/solution.py
@@ -2,6 +2,13 @@
 import jax.numpy as jnp
 from jax import lax
 from jax.sharding import PartitionSpec as P
+from jax.lax import all_gather
+
+
+def order_loops_over_axis(z_in):
+    later = all_gather(z_in, axis_name="fs")
+    u1 = jnp.concatenate(later, axis=1)
+    return u1
 
 
 def convolve(values, taps, bias):
@@ -44,7 +51,7 @@
     columns = out_grad
     grad_hidden = lax.dot_general(
         columns,
-        lax.all_gather(down_weight, "fs", axis=1, tiled=True),
+        order_loops_over_axis(down_weight),
         (((1,), (1,)), ((), ())),
         preferred_element_type=jnp.float32,
     )

time: 669 us -> 689 us (1.030)
  local copies, waits for them, and re-layouts: 8.47 us -> 19.9 us
  other arithmetic: 40.2 us -> 48.9 us
    reshape x0 -> x1, local copies, waits for them, and re-layouts: none -> 11.4 us  [order_loops_over_axis(): u1 = jnp.concatenate(later, axis=1)]
    reduce_sum x1, other arithmetic: 19 us -> 27.6 us  [local(): jnp.sum(grad_gate_pre, axis=0)]
where the time goes in v1:
time: 689 us; the launch traced here: 688 us
  waiting for transfers between devices  542 us (79%)
  other arithmetic  48.9 us (7%)
  matrix products  41.6 us (6%)
  blocking collectives  22.3 us (3%)
  local copies, waits for them, and re-layouts  19.9 us (3%)
  between operations  13.8 us (2%)
    reduce_scatter x1, waiting for transfers between devices, local(): lax.psum_scatter(lax.dot_general(columns, hidden, (((0,), (0,)), ((), ())...  279 us
    all_gather x1, waiting for transfers between devices, order_loops_over_axis(): later = all_gather(z_in, axis_name='fs')  120 us
    psum x1, waiting for transfers between devices, local(): lax.psum((conv_parts[0], conv_parts[1], conv_parts[2], conv_parts[3]), ('...  88.1 us
    psum x1, waiting for transfers between devices, local(): summed = lax.psum(partial_grad, 'rep')  54 us
    dot_general x1, matrix products, local(): lax.dot_general(columns, order_loops_over_axis(down_weight), (((1,), (1,)...  28 us
    reduce_sum x1, other arithmetic, local(): jnp.sum(grad_gate_pre, axis=0)  27.6 us
    psum x1, blocking collectives, local(): row_norms = lax.psum(jnp.sum(grad_down * grad_down, axis=1), 'fs')  22.3 us
  transfers between devices with their start and end apart: 4, of which 4 were waited for; matrix products, arithmetic and copies ran while one was open for 3% of the time, Pallas kernels for 0%

profile of v1, /device:TPU:0, one launch (start us, length us, event | category | flops | bytes accessed | tf_op | source)
XLA Modules:
  0.0 688.3 jit_solution(17979869887643094355)
XLA Ops:
  7.2 0.0 copy-start
  7.2 0.0 all-gather.3.cloned.1.call-start
  7.2 0.7 all-gather.3.cloned.1.call-update
  7.9 0.0 reduce-scatter.2.cloned.1.call-start
  8.0 0.0 copy-start.3
  8.0 5.6 convert_element_type.24
  13.5 0.0 copy-done.3
  13.5 0.0 copy-start.4
  13.5 0.0 copy-start.5
  13.5 3.5 convert_element_type.23
  17.0 0.0 copy-done.4
  17.0 0.0 copy-done.5
  17.1 120.3 %all-gather.3.cloned.1.call-done = bf16[16384,256]{1,0:T(8,128)(2,1)} async-done(((bf16[2048,256]{1,0:T(8,128)(2,1)}), bf16[16384,256]{1,0:T(8,128)(2,1)}) %all-gather.3.cloned.1.call-update) | async-done | bytes 8388624 | tf_op jit(solution)/shard_map/all_gather | solution.py:9
  137.3 0.0 copy-start.7
  137.4 11.4 %copy.16 = bf16[2048,8,256]{0,2,1:T(8,128)(2,1)} copy(bf16[2048,8,256]{2,0,1:T(8,128)(2,1)} %bitcast.22) | data formatting | bytes 16777216 | tf_op jit(solution)/shard_map/reshape | solution.py:10
  148.8 0.0 copy-done
  148.8 0.0 copy-done.7
  148.8 0.0 copy-start.1
  148.8 0.0 copy-start.6
  148.8 28.0 %fusion.4 = (f32[2048]{0:T(1024)}, f32[2048]{0:T(1024)S(1)}, f32[2048]{0:T(1024)S(1)}, f32[2048]{0:T(1024)S(1)}, f32[768,2048]{1,0:T(8,128)}, /*index=5*/f32[768,2048]{1,0:T(8,128)}, f32[768,2048]{1,0:T(8,128)}) fusion(bf16[768,2048]{1,0:T(8,128)(2,1)} %param.9, f32[768,2048]{1,0:T(8,128)} %convert_element_type.23, f32[2048]{0:T(1024)S(1)} %copy-done.7, ...), kind=kOutput, calls=%fused_computation.24 | convolution fusion | flops 6472327168 | bytes 46202880 | tf_op jit(solution)/shard_map/dot_general | solution.py:52
  176.8 0.0 copy-done.1
  176.8 0.0 copy-done.6
  176.9 0.0 copy-start.2
  176.9 27.6 %fusion.5 = (f32[2048]{0:T(1024)}, f32[2048]{0:T(1024)S(1)}, f32[2048]{0:T(1024)S(1)}, f32[2048]{0:T(1024)S(1)}, f32[768,2048]{1,0:T(8,128)}, /*index=5*/f32[768,2048]{1,0:T(8,128)}, bf16[768,2048]{1,0:T(8,128)(2,1)}) fusion(bf16[768,2048]{1,0:T(8,128)(2,1)S(1)} %copy-done.1, f32[768,2048]{1,0:T(8,128)} %convert_element_type.24, ...), kind=kLoop, calls=%fused_computation.25 | loop fusion | flops 45604864 | bytes 50397184 | tf_op jit(solution)/shard_map/reduce_sum | solution.py:65
  204.5 0.0 copy-done.2
  204.5 13.6 %convolution_bitcast_fusion = f32[2048,2048]{0,1:T(8,128)} fusion(bf16[768,2048]{1,0:T(8,128)(2,1)S(1)} %copy-done, f32[768,2048]{1,0:T(8,128)} %get-tuple-element.27, f32[768,2048]{1,0:T(8,128)S(1)} %copy-done.2), kind=kOutput, calls=%fused_computation | convolution fusion | flops 6451888128 | bytes 32505856 | tf_op jit(solution)/shard_map/dot_general | solution.py:73
  218.1 0.0 reduce-scatter.2.cloned.1.call-update
  218.1 0.0 all-reduce.8.cloned.1.call-start
  218.1 278.5 %reduce-scatter.2.cloned.1.call-done = f32[256,2048]{0,1:T(8,128)} async-done(((f32[2048,2048]{0,1:T(8,128)}), f32[256,2048]{0,1:T(8,128)}) %reduce-scatter.2.cloned.1.call-update) | async-done | bytes 2097168 | tf_op jit(solution)/shard_map/reduce_scatter | solution.py:72
  496.7 0.0 all-reduce.8.cloned.1.call-update
  496.7 0.0 all-reduce.10.cloned.1.call-start
  496.7 0.7 pad_maximum_fusion
  497.4 9.6 %add_convert_fusion.1 = bf16[768,2048]{1,0:T(8,128)(2,1)} fusion(f32[768,2048]{1,0:T(8,128)} %get-tuple-element.26, f32[2048]{0:T(1024)S(1)} %bitcast.34, f32[2048]{0:T(1024)S(1)} %bitcast.36, f32[2048]{0:T(1024)S(1)} %bitcast.32), kind=kLoop, calls=%fused_computation.9 | loop fusion | flops 9437184 | bytes 9461760 | tf_op jit(solution)/shard_map/convert_element_type | solution.py:60
  507.0 0.0 all-reduce.10.cloned.1.call-update
  507.0 54.0 %all-reduce.8.cloned.1.call-done = f32[2048,256]{1,0:T(8,128)} async-done(((f32[2048,256]{1,0:T(8,128)}), f32[2048,256]{1,0:T(8,128)}) %all-reduce.8.cloned.1.call-update) | async-done | bytes 2097168 | tf_op jit(solution)/shard_map/psum | solution.py:80
  561.1 1.9 multiply_reduce_fusion.6
  563.0 22.3 %psum.47 = f32[2048]{0:T(1024)} all-reduce(f32[2048]{0:T(1024)S(1)} %multiply_reduce_fusion.6), channel_id=1, replica_groups=mesh['rep'=2,'fs'=8,'tp'=2] {'fs'}, use_global_device_ids=true, to_apply=%region_15.16 | all-reduce | flops 2048 | bytes 16384 | tf_op jit(solution)/shard_map/psum | solution.py:82
  585.3 88.1 %all-reduce.10.cloned.1.call-done = (f32[3,2048]{1,0:T(4,128)}, f32[3,2048]{1,0:T(4,128)}, f32[2048]{0:T(1024)}, f32[2048]{0:T(1024)}) async-done(((f32[3,2048]{1,0:T(4,128)}, f32[3,2048]{1,0:T(4,128)}, f32[2048]{0:T(1024)}, f32[2048]{0:T(1024)}), (f32[3,2048]{1,0:T(4,128)}, f32[3,2048]{1,0:T(4,128)}, f32[2048]{0:T(1024)}, f32[2048]{0:T(1024)})) %all-reduce.10.cloned.1.call-update) | async-done | bytes 65552 | tf_op jit(solution)/shard_map/psum | solution.py:68
  673.4 1.4 copy.22
  674.8 1.4 copy.23
  676.2 1.3 copy.24
  677.5 1.3 copy.25
  678.8 3.0 copy.26
  (2 shorter events, 0.0 us)
Async XLA Ops:
  7.2 141.6 %copy-start = (bf16[768,2048]{1,0:T(8,128)(2,1)S(1)}, bf16[768,2048]{1,0:T(8,128)(2,1)}, u32[]{:S(2)}) copy-start(bf16[768,2048]{1,0:T(8,128)(2,1)} %param.15) | copy-start | bytes 9437188
  7.2 130.2 %all-gather.3.cloned.1.call-start = ((), (), s32[]{:S(2)}) async-start(), calls=%async_computation.3 | async-start | bytes 9437184 | tf_op jit(solution)/shard_map/all_gather | solution.py:9
  7.9 488.7 %reduce-scatter.2.cloned.1.call-start = ((), (), s32[]{:S(2)}) async-start(), calls=%async_computation.1 | async-start | bytes 18874368 | tf_op jit(solution)/shard_map/reduce_scatter | solution.py:72
  8.0 5.6 copy-start.3
  13.5 3.5 copy-start.4
  13.5 3.5 copy-start.5
  137.3 11.5 %copy-start.7 = (f32[2048]{0:T(1024)S(1)}, f32[2048]{0:T(1024)}, u32[]{:S(2)}) copy-start(f32[2048]{0:T(1024)} %param.12) | copy-start | bytes 24580
  148.8 28.0 %copy-start.1 = (bf16[768,2048]{1,0:T(8,128)(2,1)S(1)}, bf16[768,2048]{1,0:T(8,128)(2,1)}, u32[]{:S(2)}) copy-start(bf16[768,2048]{1,0:T(8,128)(2,1)} %param.8) | copy-start | bytes 9437188
  148.8 28.0 %copy-start.6 = (f32[2048]{0:T(1024)S(1)}, f32[2048]{0:T(1024)}, u32[]{:S(2)}) copy-start(f32[2048]{0:T(1024)} %param.13) | copy-start | bytes 24580
  176.9 27.6 %copy-start.2 = (f32[768,2048]{1,0:T(8,128)S(1)}, f32[768,2048]{1,0:T(8,128)}, u32[]{:S(2)}) copy-start(f32[768,2048]{1,0:T(8,128)} %get-tuple-element.25) | copy-start | bytes 18874372
  218.1 343.0 %all-reduce.8.cloned.1.call-start = ((), (), s32[]{:S(2)}) async-start(), calls=%async_computation.2 | async-start | bytes 4194304 | tf_op jit(solution)/shard_map/psum | solution.py:80
  496.7 176.7 %all-reduce.10.cloned.1.call-start = ((), (), s32[]{:S(2)}) async-start(), calls=%async_computation.4 | async-start | bytes 163840 | tf_op jit(solution)/shard_map/psum | solution.py:68
Sparse Core Ops, SparseCore 0:
  10.1 127.1 all-gather.2
  218.2 278.3 reduce-scatter.1
  498.9 62.0 all-reduce.7
  567.4 105.9 all-reduce.9
